TPU v7x, 256 devices: a 4x2x16 block of a 4x16x16 slice. The times are simulated.
256 devices in a mesh: grp: 2 (over y), sp: 16 (over z), tp: 8 (over x, core).
Axes of the slice: x: 4, y: 2, z: 16, core: 2. Of those that a mesh axis runs over, the one named last changes fastest.
The devices are a block of a 4x16x16 slice.
Arguments:
- tokens: bfloat16 [32, 4096, 4096], P(('grp', 'tp'), 'sp'), parts along dimension 0, may hold values from -8 to 8, as said below
- offsets: int32 [32], P(('grp', 'tp')), parts along dimension 0, may hold values from 0 to 4095
- in_gain: float32 [4096], replicated, may hold values from 0.1 to 1.9
- w_latent: bfloat16 [4096, 1024], P('sp'), may hold values from -0.09375 to 0.09375
- w_rope_key: bfloat16 [4096, 32], replicated, may hold values from -0.09375 to 0.09375
- kv_gain: float32 [1024], replicated, may hold values from 0.1 to 1.9
- w_up_key: bfloat16 [1024, 2048], P(None, 'tp'), may hold values from -0.1875 to 0.1875
- w_up_value: bfloat16 [1024, 2048], P(None, 'tp'), may hold values from -0.1875 to 0.1875
- q_nope: bfloat16 [32, 2048], P(('grp', 'sp'), 'tp'), parts along dimension 0, may hold values from -300 to 300, as said below
- q_rope: bfloat16 [32, 1024], P(('grp', 'sp'), 'tp'), parts along dimension 0, may hold values from -16 to 16
Outputs:
- keys: bfloat16 [32, 4096, 2048], P(('grp', 'sp'), None, 'tp'), parts along dimension 0
- values: bfloat16 [32, 4096, 2048], P(('grp', 'sp'), None, 'tp'), parts along dimension 0
- rope_keys: bfloat16 [32, 32, 4096], P(('grp', 'sp')), parts along dimension 0
- read: bfloat16 [32, 2048], P(('grp', 'sp'), 'tp'), parts along dimension 0
There are 2 independent parts, one for each index of `grp`. A program takes and returns all parts, laid end to end along the dimension named above; an argument that names none is the same for every part. Nothing has to cross between parts.
Inputs may be any that keep to these rules, and one draw needn't show every extreme that they name: `tokens`: entries of the layer's input. `q_nope`: entries of the first decoding token's queries.
All inputs are finite; a program needn't handle non-finite values.
Results may differ from a plain program's by a relative error of at most 0.02.
Values may be sent and summed in bfloat16 or wider, within the bound.
A program may use at most 128 MiB of HBM per device.

v0:
```python
import jax
import jax.numpy as jnp
from jax import lax
from jax.sharding import PartitionSpec as P

HEAD = 64
ROPE = 32


EPS = 1e-06


def joined_along(tiles, dim):
    shape = list(tiles.shape[1:])
    shape[dim] *= tiles.shape[0]
    return jnp.moveaxis(tiles, 0, dim).reshape(shape)


def copy_for_each(value, axis):
    peers = lax.axis_size(axis)
    return lax.all_to_all(
        jnp.broadcast_to(value[None], (peers, *value.shape)), axis, 0, 0, tiled=True
    )


def gather_directly(value, axis, dim):
    return joined_along(copy_for_each(value, axis), dim)


def rms_scale(values, gain):
    wide = values.astype(jnp.float32)
    return wide * lax.rsqrt(jnp.mean(wide * wide, axis=-1, keepdims=True) + EPS) * gain


def rotate(raw, position):
    inverse = 10000.0 ** (-jnp.arange(0, ROPE, 2).astype(jnp.float32) / ROPE)
    angle = position.astype(jnp.float32)[..., None] * inverse
    cosine, sine = (jnp.cos(angle), jnp.sin(angle))
    half = ROPE // 2
    first, second = (raw[..., :half], raw[..., half:])
    return jnp.concatenate(
        [first * cosine - second * sine, second * cosine + first * sine], axis=-1
    )


def local(
    tokens, offsets, in_gain, w_latent, w_rope_key, kv_gain, w_up_key, w_up_value, q_nope, q_rope
):
    prompts, rows, width = tokens.shape
    n_sp = lax.axis_size("sp")
    length = n_sp * rows
    block = lax.axis_index("sp")
    normed = rms_scale(tokens.reshape(prompts * rows, width), in_gain).astype(jnp.bfloat16)
    latent_raw = jnp.dot(
        normed,
        lax.all_gather(w_latent, "sp", axis=0, tiled=True),
        preferred_element_type=jnp.float32,
    )
    latent = rms_scale(latent_raw, kv_gain).astype(jnp.bfloat16)
    position = offsets[:, None] + block * rows + jnp.arange(rows, dtype=jnp.int32)[None, :]
    rope_raw = jnp.dot(normed, w_rope_key, preferred_element_type=jnp.float32).reshape(
        prompts, rows, ROPE
    )
    rotated = rotate(rope_raw, position).astype(jnp.bfloat16)
    head_cols = w_up_key.shape[1]
    paired = jnp.stack([w_up_key, w_up_value])
    both = jnp.einsum(
        "tk,skc->stc",
        latent,
        lax.all_gather(paired, "tp", axis=2, tiled=True),
        preferred_element_type=jnp.float32,
    ).astype(jnp.bfloat16)
    both = both.reshape(2, prompts, rows, both.shape[2])
    by_head = lax.all_to_all(both, "tp", split_axis=3, concat_axis=1, tiled=True)
    rope_every = gather_directly(rotated, "tp", 0)
    moved, rope_moved = (
        lax.all_to_all(by_head[:, :, None], "sp", split_axis=1, concat_axis=2, tiled=True),
        lax.all_to_all(rope_every[None, :, None], "sp", split_axis=1, concat_axis=2, tiled=True),
    )
    keys = moved[0].reshape(length, head_cols)
    values = moved[1].reshape(length, head_cols)
    rope_all = rope_moved.reshape(length, ROPE)
    rope_keys = rope_all.T
    heads_here = head_cols // HEAD
    query = q_nope.reshape(heads_here, HEAD)
    rotary_q = q_rope.reshape(heads_here, ROPE)
    keys_split = keys.reshape(length, heads_here, HEAD)
    scores = jnp.einsum("hd,jhd->hj", query, keys_split, preferred_element_type=jnp.float32)
    scores = scores + jnp.dot(rotary_q, rope_keys, preferred_element_type=jnp.float32)
    scores = scores / jnp.sqrt(jnp.float32(HEAD + ROPE))
    peak = jnp.max(scores, axis=-1, keepdims=True)
    expo = jnp.exp(scores - peak)
    weights = (expo / jnp.sum(expo, axis=-1, keepdims=True)).astype(jnp.bfloat16)
    read = jnp.einsum(
        "hj,jhd->hd",
        weights,
        values.reshape(length, heads_here, HEAD),
        preferred_element_type=jnp.float32,
    )
    read = read.astype(jnp.bfloat16).reshape(1, heads_here * HEAD)
    return (keys[None], values[None], rope_keys[None], read)


def solution(mesh):
    in_specs = (
        P(("grp", "tp"), "sp", None),
        P(("grp", "tp")),
        P(),
        P("sp", None),
        P(),
        P(),
        P(None, "tp"),
        P(None, "tp"),
        P(("grp", "sp"), "tp"),
        P(("grp", "sp"), "tp"),
    )
    out_specs = (
        P(("grp", "sp"), None, "tp"),
        P(("grp", "sp"), None, "tp"),
        P(("grp", "sp"), None, None),
        P(("grp", "sp"), "tp"),
    )
    return jax.shard_map(local, mesh=mesh, in_specs=in_specs, out_specs=out_specs, check_vma=False)
```

profile of v0, /device:TPU:163, one launch (start us, length us, event | category | flops | bytes accessed | tf_op | source)
XLA Modules:
  0.0 513.6 jit_solution(11231751343885072324)
XLA Ops:
  7.2 0.0 copy-start
  7.2 0.1 all-gather.5.cloned.1.call-start
  7.3 0.7 all-gather.5.cloned.1.call-update
  8.0 0.1 all-gather.3.cloned.1.call-start
  8.1 2.3 pad_maximum_fusion
  10.3 0.1 all-gather.3.cloned.1.call-update
  10.4 0.0 copy-start.3
  10.4 0.8 broadcast_add_fusion
  11.2 0.1 add_convert_fusion
  11.3 3.3 multiply_reduce_fusion
  14.7 1.4 fusion.4
  16.1 0.2 fusion.21
  16.4 0.8 broadcast_in_dim.7
  17.2 5.2 %all-to-all-start.2 = ((bf16[8,2,256,32]{2,1,3,0:T(2,128)(2,1)}), bf16[8,2,256,32]{2,1,3,0:T(2,128)(2,1)S(1)}, u32[]{:S(2)}, u32[]{:S(2)}) async-start(bf16[8,2,256,32]{2,1,3,0:T(2,128)(2,1)} %broadcast_in_dim.7), calls=%async_computation.2 | async-start | bytes 524288 | tf_op jit(solution)/shard_map/all_to_all | solution.py:21
  22.4 5.8 %fusion.1 = bf16[512,4096]{1,0:T(8,128)(2,1)} fusion(bf16[2,256,4096]{2,1,0:T(8,128)(2,1)} %param.10, f32[4096]{0:T(1024)S(1)} %copy-done.6, f32[512]{0:T(512)S(1)} %bitcast.76), kind=kLoop, calls=%fused_computation.2 | loop fusion | flops 8388608 | bytes 8407040 | tf_op jit(solution)/shard_map/convert_element_type | solution.py:53
  28.2 95.7 %all-gather.5.cloned.1.call-done = bf16[4096,1024]{1,0:T(8,128)(2,1)} async-done(((bf16[256,1024]{1,0:T(8,128)(2,1)}), bf16[4096,1024]{1,0:T(8,128)(2,1)}) %all-gather.5.cloned.1.call-update) | async-done | bytes 8388624 | tf_op jit(solution)/shard_map/all_gather | solution.py:56
  123.8 8.3 %multiply_reduce_fusion.1 = (f32[512]{0:T(512)S(1)}, f32[512,1024]{1,0:T(8,128)S(1)}) fusion(bf16[512,4096]{1,0:T(8,128)(2,1)} %fusion.1, bf16[4096,1024]{1,0:T(8,128)(2,1)} %all-gather.5.cloned.1.call-done), kind=kOutput, calls=%fused_computation.14 | convolution fusion | flops 4296015360 | bytes 14682112 | tf_op jit(solution)/shard_map/dot_general | solution.py:54
  132.1 54.6 %all-gather.3.cloned.1.call-done = bf16[2,1024,2048]{2,1,0:T(8,128)(2,1)} async-done(((bf16[2,1024,256]{2,1,0:T(8,128)(2,1)}), bf16[2,1024,2048]{2,1,0:T(8,128)(2,1)}) %all-gather.3.cloned.1.call-update) | async-done | bytes 8388624 | tf_op jit(solution)/shard_map/all_gather | solution.py:70
  186.7 9.6 %convolution_convert_fusion = bf16[2,2048,512]{1,2,0:T(8,128)(2,1)} fusion(bf16[2,1024,2048]{2,1,0:T(8,128)(2,1)} %all-gather.3.cloned.1.call-done, f32[512,1024]{1,0:T(8,128)S(1)} %get-tuple-element.11, f32[1024]{0:T(1024)S(1)} %copy-done.8, f32[512]{0:T(512)S(1)} %add_rsqrt_fusion), kind=kOutput, calls=%fused_computation.12 | convolution fusion | flops 4298637312 | bytes 14686208 | tf_op jit(solution)/shard_map/tk,skc->stc/dot_general | solution.py:67
  196.4 11.2 %copy.25 = bf16[2,2,256,2048]{2,1,0,3:T(2,128)(2,1)} copy(bf16[2,2,256,2048]{3,2,1,0:T(8,128)(2,1)} %bitcast.68) | data formatting | bytes 8388608 | tf_op jit(solution)/shard_map/reshape | solution.py:73
  207.5 4.9 all-to-all-start
  212.4 0.7 copy.30
  213.2 47.1 %all-to-all-done = bf16[2,2,256,2048]{2,1,0,3:T(2,128)(2,1)} async-done(((bf16[2,2,256,2048]{2,1,0,3:T(2,128)(2,1)}), bf16[2,2,256,2048]{2,1,0,3:T(2,128)(2,1)}, u32[]{:S(2)}, u32[]{:S(2)}) %all-to-all-start) | async-done | bytes 4194336 | tf_op jit(solution)/shard_map/all_to_all | solution.py:74
  260.2 12.0 %all-to-all-start.3 = ((bf16[1,16,1,256,32]{3,4,2,0,1:T(8,128)(2,1)}), bf16[1,16,1,256,32]{3,4,2,0,1:T(8,128)(2,1)S(1)}, u32[]{:S(2)}, u32[]{:S(2)}) async-start(bf16[1,16,1,256,32]{3,4,2,0,1:T(8,128)(2,1)} %bitcast.13), calls=%async_computation.3 | async-start | bytes 524288 | tf_op jit(solution)/shard_map/all_to_all | solution.py:78
  272.2 4.9 copy.26
  277.2 12.7 %all-to-all-done.3 = bf16[1,16,1,256,32]{3,4,2,0,1:T(8,128)(2,1)S(1)} async-done(((bf16[1,16,1,256,32]{3,4,2,0,1:T(8,128)(2,1)}), bf16[1,16,1,256,32]{3,4,2,0,1:T(8,128)(2,1)S(1)}, u32[]{:S(2)}, u32[]{:S(2)}) %all-to-all-start.3) | async-done | bytes 262176 | tf_op jit(solution)/shard_map/all_to_all | solution.py:78
  289.9 6.6 %all-to-all-start.1 = ((bf16[2,16,1,256,256]{3,4,2,0,1:T(8,128)(2,1)}), bf16[2,16,1,256,256]{3,4,2,0,1:T(8,128)(2,1)}, u32[]{:S(2)}, u32[]{:S(2)}) async-start(bf16[2,16,1,256,256]{3,4,2,0,1:T(8,128)(2,1)} %bitcast.67), calls=%async_computation.1 | async-start | bytes 8388608 | tf_op jit(solution)/shard_map/all_to_all | solution.py:77
  296.5 0.1 reshape.142
  296.6 0.5 broadcast.98
  297.1 0.7 reduce.5
  297.8 0.1 reshape.132
  297.9 0.0 copy-start.5
  297.9 181.5 %all-to-all-done.1 = bf16[2,16,1,256,256]{3,4,2,0,1:T(8,128)(2,1)} async-done(((bf16[2,16,1,256,256]{3,4,2,0,1:T(8,128)(2,1)}), bf16[2,16,1,256,256]{3,4,2,0,1:T(8,128)(2,1)}, u32[]{:S(2)}, u32[]{:S(2)}) %all-to-all-start.1) | async-done | bytes 4194336 | tf_op jit(solution)/shard_map/all_to_all | solution.py:77
  479.4 2.6 fusion.26
  481.9 0.0 copy-start.2
  482.0 1.3 copy-done.2
  483.3 2.5 copy.34
  485.8 3.9 copy.40
  489.7 2.5 copy.33
  492.2 2.4 copy.39
  494.6 4.3 reshape_reshape_squeeze.6
  498.9 2.0 fusion.28
  500.9 0.3 fusion.27
  501.1 0.2 fusion.15
  501.4 0.1 fusion.24
  501.5 2.3 reshape_reshape_squeeze.7
  503.8 2.2 fusion.13
  506.1 0.7 reshape.133
  (25 shorter events, 0.1 us)
Async XLA Ops:
  7.2 7.4 %copy-start = (bf16[4096,32]{0,1:T(8,128)(2,1)S(1)}, bf16[4096,32]{0,1:T(8,128)(2,1)}, u32[]{:S(2)}) copy-start(bf16[4096,32]{0,1:T(8,128)(2,1)} %param.14) | copy-start | bytes 786436
  7.2 7.4 %copy-start.6 = (f32[4096]{0:T(1024)S(1)}, f32[4096]{0:T(1024)}, u32[]{:S(2)}) copy-start(f32[4096]{0:T(1024)} %param.12) | copy-start | bytes 49156
  7.2 116.6 %all-gather.5.cloned.1.call-start = ((), (), s32[]{:S(2)}) async-start(), calls=%async_computation.5 | async-start | bytes 8912896 | tf_op jit(solution)/shard_map/all_gather | solution.py:56
  8.0 178.7 %all-gather.3.cloned.1.call-start = ((), (), s32[]{:S(2)}) async-start(), calls=%async_computation.4 | async-start | bytes 9437184 | tf_op jit(solution)/shard_map/all_gather | solution.py:70
  10.4 4.2 copy-start.3
  17.2 190.3 %all-to-all-start.2 = ((bf16[8,2,256,32]{2,1,3,0:T(2,128)(2,1)}), bf16[8,2,256,32]{2,1,3,0:T(2,128)(2,1)S(1)}, u32[]{:S(2)}, u32[]{:S(2)}) async-start(bf16[8,2,256,32]{2,1,3,0:T(2,128)(2,1)} %broadcast_in_dim.7), calls=%async_computation.2 | async-start | bytes 524288 | tf_op jit(solution)/shard_map/all_to_all | solution.py:21
  28.2 158.6 %copy-start.8 = (f32[1024]{0:T(1024)S(1)}, f32[1024]{0:T(1024)}, u32[]{:S(2)}) copy-start(f32[1024]{0:T(1024)} %param.15) | copy-start | bytes 12292
  207.5 52.7 %all-to-all-start = ((bf16[2,2,256,2048]{2,1,0,3:T(2,128)(2,1)}), bf16[2,2,256,2048]{2,1,0,3:T(2,128)(2,1)}, u32[]{:S(2)}, u32[]{:S(2)}) async-start(bf16[2,2,256,2048]{2,1,0,3:T(2,128)(2,1)} %copy.25), calls=%async_computation | async-start | bytes 8388608 | tf_op jit(solution)/shard_map/all_to_all | solution.py:74
  260.2 29.6 %all-to-all-start.3 = ((bf16[1,16,1,256,32]{3,4,2,0,1:T(8,128)(2,1)}), bf16[1,16,1,256,32]{3,4,2,0,1:T(8,128)(2,1)S(1)}, u32[]{:S(2)}, u32[]{:S(2)}) async-start(bf16[1,16,1,256,32]{3,4,2,0,1:T(8,128)(2,1)} %bitcast.13), calls=%async_computation.3 | async-start | bytes 524288 | tf_op jit(solution)/shard_map/all_to_all | solution.py:78
  289.9 6.6 %copy-start.7 = (bf16[1,256]{1,0:T(2,128)(2,1)S(1)}, bf16[1,256]{1,0:T(2,128)(2,1)}, u32[]{:S(2)}) copy-start(bf16[1,256]{1,0:T(2,128)(2,1)} %param.18) | copy-start | bytes 1540
  289.9 7.2 %copy-start.9 = (bf16[1,128]{1,0:T(2,128)(2,1)S(1)}, bf16[1,128]{1,0:T(2,128)(2,1)}, u32[]{:S(2)}) copy-start(bf16[1,128]{1,0:T(2,128)(2,1)} %param.19) | copy-start | bytes 772
  289.9 189.5 %all-to-all-start.1 = ((bf16[2,16,1,256,256]{3,4,2,0,1:T(8,128)(2,1)}), bf16[2,16,1,256,256]{3,4,2,0,1:T(8,128)(2,1)}, u32[]{:S(2)}, u32[]{:S(2)}) async-start(bf16[2,16,1,256,256]{3,4,2,0,1:T(8,128)(2,1)} %bitcast.67), calls=%async_computation.1 | async-start | bytes 8388608 | tf_op jit(solution)/shard_map/all_to_all | solution.py:77
  297.9 203.0 %copy-start.5 = (bf16[4,8,16,256]{3,1,2,0:T(8,128)(2,1)}, bf16[4,8,16,256]{3,1,2,0:T(8,128)(2,1)S(1)}, u32[]{:S(2)}) copy-start(bf16[4,8,16,256]{3,1,2,0:T(8,128)(2,1)S(1)} %copy.44) | copy-start | bytes 786436
  481.9 1.3 copy-start.2
  494.6 6.9 %copy-start.4 = (bf16[1,16,1,256,256]{3,1,4,2,0:T(8,128)(2,1)S(1)}, bf16[1,16,1,256,256]{3,1,4,2,0:T(8,128)(2,1)}, u32[]{:S(2)}) copy-start(bf16[1,16,1,256,256]{3,1,4,2,0:T(8,128)(2,1)} %copy.34) | copy-start | bytes 6291460
  494.6 12.2 %copy-start.1 = (bf16[4096,32]{0,1:T(8,128)(2,1)S(1)}, bf16[4096,32]{0,1:T(8,128)(2,1)}, u32[]{:S(2)}) copy-start(bf16[4096,32]{0,1:T(8,128)(2,1)} %param.14) | copy-start | bytes 786436
Sparse Core Ops, SparseCore 0:
  9.8 113.9 all-gather.4
  126.2 60.4 all-gather.2
where the time goes:
time: 517 us; the launch traced here: 514 us
  waiting for transfers between devices  392 us (76%)
  local copies, waits for them, and re-layouts  41 us (8%)
  starting transfers between devices  28.8 us (6%)
  matrix products  23.8 us (5%)
  between operations  14.2 us (3%)
  other arithmetic  13.5 us (3%)
    all_to_all x1, waiting for transfers between devices, local(): lax.all_to_all(by_head[:, :, None], 'sp', split_axis=1, concat_axis=2, ti...  181 us
    all_gather x1, waiting for transfers between devices, local(): lax.all_gather(w_latent, 'sp', axis=0, tiled=True)  95.7 us
    all_gather x1, waiting for transfers between devices, local(): lax.all_gather(paired, 'tp', axis=2, tiled=True)  54.6 us
    all_to_all x1, waiting for transfers between devices, local(): lax.all_to_all(both, 'tp', split_axis=3, concat_axis=1, tiled=True)  47.1 us
    all_to_all x1, waiting for transfers between devices, local(): lax.all_to_all(rope_every[None, :, None], 'sp', split_axis=1, concat_axis...  12.7 us
    all_to_all x1, starting transfers between devices, local(): lax.all_to_all(rope_every[None, :, None], 'sp', split_axis=1, concat_axis...  12 us
    reshape x1, local copies, waits for them, and re-layouts, local(): both = both.reshape(2, prompts, rows, both.shape[2])  11.2 us
  transfers between devices with their start and end apart: 6, of which 5 were waited for; matrix products, arithmetic and copies ran while one was open for 10% of the time, Pallas kernels for 0%

commit v1 on v0

v1 whole, which is shorter than its diff:
```python
import functools

import jax
import jax.numpy as jnp
from jax import lax
from jax.experimental import pallas as pl
from jax.experimental.pallas import tpu as pltpu
from jax.sharding import PartitionSpec as P

HEAD = 64
ROPE = 32
EPS = 1e-06
MESH = pl.DeviceIdType.MESH
FULL = 48

DO_W = True
DO_L = True
DO_C = True


def exchange(
    n_sp, n_tp, tok_hbm, off_ref, gain_ref, wl_hbm, wrope_ref, kvg_ref, wk_hbm, wv_hbm,
    keys_ref, values_ref, rope_ref,
    norm, wfull, wup, lat, acc, latall, ropeown,
    local_sem, wz_sem, wx_sem, wp_sem, wsend, dir_sem, lx_sem, lp_sem, lsend, rsem, rsend,
):
    z = lax.axis_index("sp")
    t = lax.axis_index("tp")
    n_x = n_tp // 2
    x, c = t // 2, lax.rem(t, 2)
    rows = norm.shape[0] // 2
    width = norm.shape[1]
    rank = lat.shape[1]
    depth = width // n_sp
    half = depth // 2
    quarter = rank // n_x
    piece = rows // n_x
    heads = keys_ref.shape[1]

    def wrap(v, n):
        return lax.rem(v + 2 * n, n)

    def dev(xx, cc, zz):
        return {"sp": zz, "tp": 2 * xx + cc}

    z_next, z_prev = wrap(z + 1, n_sp), wrap(z - 1, n_sp)
    right = dev(wrap(x + 1, n_x), c, z)
    left = dev(wrap(x - 1, n_x), c, z)
    up = dev(x, c, z_next)
    down = dev(x, c, z_prev)
    partner = dev(x, 1 - c, z)
    home = lax.rem(z, 2)
    has_self = jnp.logical_and(t == z // 2, c == home)

    loads = [
        pltpu.make_async_copy(wl_hbm, wfull.at[pl.ds(z * depth, depth)], local_sem.at[0]),
        pltpu.make_async_copy(tok_hbm, norm, local_sem.at[1]),
        pltpu.make_async_copy(wk_hbm, wup.at[:, pl.ds(0, heads)], local_sem.at[2]),
        pltpu.make_async_copy(wv_hbm, wup.at[:, pl.ds(heads, heads)], local_sem.at[3]),
    ]
    for load in loads:
        load.start()

    barrier = pltpu.get_barrier_semaphore()

    def greet(device):
        pl.semaphore_signal(barrier, inc=1, device_id=device, device_id_type=MESH)

    for dx in range(n_x):
        for dc in range(2):
            if dx or dc:
                greet(dev(wrap(x + dx, n_x), lax.rem(c + dc, 2), z))
    greet(up)
    greet(down)
    dests = [(j, q) for j in range(2) for q in range(n_x)]
    src_x, src_c = z // 4, lax.rem(z // 2, 2)
    for j, q in dests:
        own = jnp.logical_and(has_self, jnp.logical_and(2 * t + j == z, x == q))
        pl.when(jnp.logical_not(own))(functools.partial(greet, dev(jnp.int32(q), home, 2 * t + j)))
    for i in range(n_sp // 2):
        own = jnp.logical_and(has_self, 2 * i + c == z)
        pl.when(jnp.logical_not(own))(functools.partial(greet, dev(src_x, src_c, 2 * i + c)))
    pl.semaphore_wait(barrier, 2 * n_x - 1 + 2 + 2 * n_x + n_sp // 2 - 2 * has_self.astype(jnp.int32))

    def send(src, dst, device, send_sem, recv_sem):
        pltpu.make_async_remote_copy(
            src_ref=src, dst_ref=dst, send_sem=send_sem, recv_sem=recv_sem,
            device_id=device, device_id_type=MESH,
        ).start()

    def arrived(dst, recv_sem):
        pltpu.make_async_copy(dst, dst, recv_sem).wait()

    def w_full(s):
        return wfull.at[pl.ds(s * depth + c * half, FULL)]

    def w_part(s, xx):
        return wfull.at[
            pl.ds(s * depth + c * half + FULL, half - FULL), pl.ds(pl.multiple_of(xx * quarter, quarter), quarter)
        ]

    def w_half(s, cc):
        return wfull.at[pl.ds(s * depth + cc * half, half)]

    steps = n_sp // 2
    limit = {("f", 1): steps, ("f", -1): steps - 1, ("q", 1): steps - 1, ("q", -1): steps}

    def z_send(kind, sign, k):
        s = wrap(z - sign * k, n_sp)
        ref = w_full(s) if kind == "f" else w_part(s, x)
        row = ("f", "q").index(kind) * 2 + (sign < 0)
        send(ref, ref, up if sign > 0 else down, wsend.at[row], wz_sem.at[row, k])

    def z_arrive(kind, sign, k):
        s = wrap(z - sign * k, n_sp)
        ref = w_full(s) if kind == "f" else w_part(s, x)
        row = ("f", "q").index(kind) * 2 + (sign < 0)
        arrived(ref, wz_sem.at[row, k - 1])
        if k < limit[kind, sign]:
            z_send(kind, sign, k)
        if kind == "q":
            col = k - 1 if sign > 0 else steps + k - 2
            send(ref, ref, right, wsend.at[4], wx_sem.at[0, col])
            send(ref, ref, left, wsend.at[5], wx_sem.at[1, col])

    def x_arrive(sign, k):
        s = wrap(z - sign * k, n_sp)
        col = k - 1 if sign > 0 else steps + k - 2
        from_left, from_right = w_part(s, wrap(x - 1, n_x)), w_part(s, wrap(x + 1, n_x))
        arrived(from_left, wx_sem.at[0, col])
        if sign > 0:
            send(from_left, from_left, right, wsend.at[6], wx_sem.at[2, col])
        arrived(from_right, wx_sem.at[1, col])
        if sign < 0:
            send(from_right, from_right, left, wsend.at[6], wx_sem.at[2, col])

    def far_arrive(sign, k):
        s = wrap(z - sign * k, n_sp)
        col = k - 1 if sign > 0 else steps + k - 2
        far = w_part(s, wrap(x + 2, n_x))
        arrived(far, wx_sem.at[2, col])
        ref = w_half(s, c)
        send(ref, ref, partner, wsend.at[7], wp_sem.at[col])

    loads[0].wait()
    if DO_W:
        for kind in ("f", "q"):
            for sign in (1, -1):
                z_send(kind, sign, 0)

    loads[1].wait()

    @pl.loop(0, 2 * rows // 16)
    def _(n):
        r = pl.ds(pl.multiple_of(n * 16, 16), 16)
        wide = norm[r, :].astype(jnp.float32)
        scale = lax.rsqrt(jnp.sum(wide * wide, axis=-1, keepdims=True) * (1.0 / width) + EPS)
        norm[r, :] = (wide * scale * gain_ref[...]).astype(jnp.bfloat16)

    raw = lax.dot_general(
        wrope_ref[...], norm[...], (((1,), (1,)), ((), ())), preferred_element_type=jnp.float32
    )
    index = lax.broadcasted_iota(jnp.int32, (ROPE // 2, rows), 0).astype(jnp.float32) * 2.0
    inverse = jnp.exp(index * (-jnp.log(jnp.float32(10000.0)) / ROPE))
    place = lax.broadcasted_iota(jnp.int32, (ROPE // 2, rows), 1)
    for j in range(2):
        angle = (off_ref[j] + z * rows + place).astype(jnp.float32) * inverse
        cosine, sine = jnp.cos(angle), jnp.sin(angle)
        first = raw[: ROPE // 2, j * rows:(j + 1) * rows]
        second = raw[ROPE // 2:, j * rows:(j + 1) * rows]
        ropeown[j] = jnp.concatenate(
            [first * cosine - second * sine, second * cosine + first * sine], axis=0
        ).astype(jnp.bfloat16)

    column = lax.rem(z // 2, n_x)
    for j in range(2):
        own = jnp.logical_and(has_self, jnp.logical_and(2 * t + j == z, x == column))
        dst = rope_ref.at[:, pl.ds(pl.multiple_of(z * rows, rows), rows)]

        @pl.when(own)
        def _():
            pltpu.make_async_copy(ropeown.at[j], dst, rsem.at[z]).start()

        @pl.when(jnp.logical_not(own))
        def _():
            send(ropeown.at[j], dst, dev(column, home, 2 * t + j), rsend.at[0, j], rsem.at[z])

    if DO_W:
        for k in range(1, steps + 1):
            for sign in (1, -1):
                for kind in ("q", "f"):
                    if k <= limit[kind, sign]:
                        z_arrive(kind, sign, k)
            for sign in (1, -1):
                if 1 <= k - 1 <= limit["q", sign]:
                    x_arrive(sign, k - 1)
            for sign in (1, -1):
                if 1 <= k - 2 <= limit["q", sign]:
                    far_arrive(sign, k - 2)
        x_arrive(-1, steps)
        for sign in (1, -1):
            far_arrive(sign, steps - 1)
        far_arrive(-1, steps)
        for sign in (1, -1):
            for k in range(1, limit["q", sign] + 1):
                col = k - 1 if sign > 0 else steps + k - 2
                arrived(w_half(wrap(z - sign * k, n_sp), 1 - c), wp_sem.at[col])

    def rope_block(s):
        return rope_ref.at[:, pl.ds(pl.multiple_of(s * rows, rows), rows)]

    peers = [(dx, dc) for dx in range(n_x) for dc in range(2) if dx or dc]
    for g in range(n_sp // 2 // n_x):
        s = 2 * (x + n_x * g) + c
        arrived(rope_block(s), rsem.at[s])
        for n, (dx, dc) in enumerate(peers):
            send(
                rope_block(s), rope_block(s), dev(wrap(x + dx, n_x), lax.rem(c + dc, 2), z),
                rsend.at[1 + g, n], rsem.at[s],
            )

    def own_piece(j, q):
        return lat.at[pl.ds(j * rows + q * piece, piece)]

    def place_of(s, q):
        return latall.at[pl.ds(pl.multiple_of(s * rows + q * piece, piece), piece)]

    for j in range(2):
        if DO_C:
            @pl.loop(0, n_x)
            def _(n):
                cols = pl.ds(pl.multiple_of(n * quarter, quarter), quarter)
                acc[:, cols] = jnp.dot(
                    norm[j * rows:(j + 1) * rows, :], wfull[:, cols], preferred_element_type=jnp.float32
                )

        @pl.loop(0, rows // 16)
        def _(n):
            r = pl.ds(pl.multiple_of(n * 16, 16), 16)
            wide = acc[r, :]
            scale = lax.rsqrt(jnp.sum(wide * wide, axis=-1, keepdims=True) * (1.0 / rank) + EPS)
            lat[pl.ds(pl.multiple_of(j * rows + n * 16, 16), 16), :] = (wide * scale * kvg_ref[...]).astype(
                jnp.bfloat16
            )

        if DO_L:
            for d in range(n_x):
                q = wrap(x + d, n_x)
                own = jnp.logical_and(has_self, 2 * t + j == z) if d == 0 else False
                src, dst = own_piece(j, q), place_of(z, q)

                def remote(src=src, dst=dst, q=q):
                    send(src, dst, dev(q, home, 2 * t + j), lsend.at[0, j], dir_sem.at[z // 2])

                if d == 0:
                    pl.when(own)(
                        lambda src=src, dst=dst: pltpu.make_async_copy(src, dst, dir_sem.at[z // 2]).start()
                    )
                    pl.when(jnp.logical_not(own))(remote)
                else:
                    remote()

    near = [0] + [v for k in range(2, steps, 2) for v in (k, -k)] + [steps]
    odd = [v for k in range(1, steps, 2) for v in (k, -k)]
    same = home == c
    sources = [wrap(z + jnp.where(same, a, b), n_sp) for a, b in zip(near, odd)]
    n_src = len(sources)

    def direct(n):
        s = sources[n]
        ref = place_of(s, x)
        arrived(ref, dir_sem.at[s // 2])
        send(ref, ref, right, lsend.at[1, 0], lx_sem.at[0, n])
        send(ref, ref, left, lsend.at[1, 1], lx_sem.at[1, n])

    def beside(n):
        s = sources[n]
        from_left, from_right = place_of(s, wrap(x - 1, n_x)), place_of(s, wrap(x + 1, n_x))
        arrived(from_left, lx_sem.at[0, n])
        if n % 2 == 0:
            send(from_left, from_left, right, lsend.at[2, 0], lx_sem.at[2, n])
        arrived(from_right, lx_sem.at[1, n])
        if n % 2 == 1:
            send(from_right, from_right, left, lsend.at[2, 0], lx_sem.at[2, n])

    def block(s):
        return latall.at[pl.ds(pl.multiple_of(s * rows, rows), rows)]

    def far(n):
        s = sources[n]
        arrived(place_of(s, wrap(x + 2, n_x)), lx_sem.at[2, n])
        send(block(s), block(s), partner, lsend.at[2, 1], lp_sem.at[s])

    def up_project(s):
        r = pl.ds(pl.multiple_of(s * rows, rows), rows)
        both = jnp.dot(latall[r, :], wup[...], preferred_element_type=jnp.float32).astype(jnp.bfloat16)
        keys_ref[r, :] = both[:, :heads]
        values_ref[r, :] = both[:, heads:]

    loads[2].wait()
    loads[3].wait()
    if DO_L:
        for n in range(n_src + 2):
            if n < n_src:
                direct(n)
            if 1 <= n <= n_src:
                beside(n - 1)
            if 2 <= n:
                far(n - 2)
        other = [wrap(z + jnp.where(same, b, a), n_sp) for a, b in zip(near, odd)]
        for n in range(n_src):
            arrived(block(other[n]), lp_sem.at[other[n]])
    if DO_C:
        @pl.loop(0, n_sp)
        def _(s):
            up_project(s)

    for s in range(n_sp):
        mine = jnp.logical_and(lax.rem(s // 2, n_x) == x, s % 2 == c)

        @pl.when(jnp.logical_not(mine))
        def _():
            arrived(rope_block(s), rsem.at[s])

    for j in range(2):
        own = jnp.logical_and(has_self, jnp.logical_and(2 * t + j == z, x == column))

        @pl.when(jnp.logical_not(own))
        def _():
            arrived(ropeown.at[j], rsend.at[0, j])

    for g in range(n_sp // 2 // n_x):
        for n in range(len(peers)):
            arrived(ropeown.at[0], rsend.at[1 + g, n])
    if DO_W:
        for sign in (1, -1):
            for _ in range(1):
                f_rows, q_rows = limit["f", sign] * FULL, limit["q", sign] * (half - FULL)
                arrived(wfull.at[pl.ds(0, f_rows)], wsend.at[int(sign < 0)])
                arrived(wfull.at[pl.ds(0, q_rows), pl.ds(0, quarter)], wsend.at[2 + int(sign < 0)])
        q_rows = (2 * steps - 1) * (half - FULL)
        for row in (4, 5, 6):
            arrived(wfull.at[pl.ds(0, q_rows), pl.ds(0, quarter)], wsend.at[row])
        arrived(wfull.at[pl.ds(0, (2 * steps - 1) * half)], wsend.at[7])
    if DO_L:
        for j in range(2):
            own = jnp.logical_and(has_self, 2 * t + j == z)
            pl.when(own)(lambda: arrived(lat.at[pl.ds(0, rows - piece)], lsend.at[0, j]))
            pl.when(jnp.logical_not(own))(lambda: arrived(lat.at[pl.ds(0, rows)], lsend.at[0, j]))
        for a, b in ((1, 0), (1, 1), (2, 0)):
            arrived(latall.at[pl.ds(0, n_src * piece)], lsend.at[a, b])
        arrived(latall.at[pl.ds(0, n_src * rows)], lsend.at[2, 1])


def attend(
    keys_ref, values_ref, rope_ref, qn_ref, qr_ref, keys_out, values_out, rope_out, read_ref, sem
):
    outs = [
        pltpu.make_async_copy(keys_ref, keys_out, sem.at[0]),
        pltpu.make_async_copy(values_ref, values_out, sem.at[1]),
        pltpu.make_async_copy(rope_ref, rope_out, sem.at[2]),
    ]
    for out in outs:
        out.start()
    heads = keys_ref.shape[1] // HEAD
    rot = qr_ref.shape[1] // heads
    pad = 8

    def by_head(ref, size):
        wide = jnp.broadcast_to(ref[...].astype(jnp.float32), (pad, ref.shape[1]))
        row = lax.broadcasted_iota(jnp.int32, wide.shape, 0)
        col = lax.broadcasted_iota(jnp.int32, wide.shape, 1)
        return jnp.where(col // size == row, wide, 0.0)

    nope = by_head(qn_ref, HEAD).astype(jnp.bfloat16)
    scores = lax.dot_general(
        nope, keys_ref[...], (((1,), (1,)), ((), ())), preferred_element_type=jnp.float32
    )
    spread = by_head(qr_ref, rot)
    rotary = spread[:, :rot]
    for h in range(1, heads):
        rotary = rotary + spread[:, h * rot:(h + 1) * rot]
    scores = scores + jnp.dot(
        rotary.astype(jnp.bfloat16), rope_ref[...], preferred_element_type=jnp.float32
    )
    scores = scores / jnp.sqrt(jnp.float32(HEAD + ROPE))
    expo = jnp.exp(scores - jnp.max(scores, axis=-1, keepdims=True))
    weights = (expo / jnp.sum(expo, axis=-1, keepdims=True)).astype(jnp.bfloat16)
    read = jnp.dot(weights, values_ref[...], preferred_element_type=jnp.float32)
    row = lax.broadcasted_iota(jnp.int32, read.shape, 0)
    col = lax.broadcasted_iota(jnp.int32, read.shape, 1)
    read_ref[...] = jnp.sum(
        jnp.where(col // HEAD == row, read, 0.0), axis=0, keepdims=True
    ).astype(jnp.bfloat16)
    for out in outs:
        out.wait()


def local(
    n_sp, n_tp,
    tokens, offsets, in_gain, w_latent, w_rope_key, kv_gain, w_up_key, w_up_value, q_nope, q_rope
):
    prompts, rows, width = tokens.shape
    depth, rank = w_latent.shape
    heads = w_up_key.shape[1]
    length = n_sp * rows
    steps = n_sp // 2
    any_space = pl.BlockSpec(memory_space=pl.ANY)
    vmem = pl.BlockSpec(memory_space=pltpu.VMEM)
    smem = pl.BlockSpec(memory_space=pltpu.SMEM)
    dma = pltpu.SemaphoreType.DMA
    keys, values, rope = pl.pallas_call(
        functools.partial(exchange, n_sp, n_tp),
        out_shape=(
            jax.ShapeDtypeStruct((length, heads), jnp.bfloat16),
            jax.ShapeDtypeStruct((length, heads), jnp.bfloat16),
            jax.ShapeDtypeStruct((ROPE, length), jnp.bfloat16),
        ),
        in_specs=[any_space, smem, vmem, any_space, vmem, vmem, any_space, any_space],
        out_specs=(vmem, vmem, vmem),
        scratch_shapes=[
            pltpu.VMEM((prompts * rows, width), jnp.bfloat16),
            pltpu.VMEM((width, rank), jnp.bfloat16),
            pltpu.VMEM((rank, 2 * heads), jnp.bfloat16),
            pltpu.VMEM((prompts * rows, rank), jnp.bfloat16),
            pltpu.VMEM((rows, rank), jnp.float32),
            pltpu.VMEM((length, rank), jnp.bfloat16),
            pltpu.VMEM((prompts, ROPE, rows), jnp.bfloat16),
            dma((4,)),
            dma((4, steps)),
            dma((3, 2 * steps - 1)),
            dma((2 * steps - 1,)),
            dma((8,)),
            dma((steps,)),
            dma((3, steps)),
            dma((n_sp,)),
            dma((3, 2)),
            dma((n_sp,)),
            dma((1 + n_sp // n_tp, n_tp - 1)),
        ],
        compiler_params=pltpu.CompilerParams(
            collective_id=0, has_side_effects=True, vmem_limit_bytes=48 * 1024 * 1024
        ),
        name="exchange",
    )(
        tokens.reshape(prompts * rows, width), offsets, in_gain.reshape(1, width), w_latent,
        w_rope_key.T, kv_gain.reshape(1, rank), w_up_key, w_up_value,
    )
    return pl.pallas_call(
        attend,
        out_shape=(
            jax.ShapeDtypeStruct((length, heads), jnp.bfloat16),
            jax.ShapeDtypeStruct((length, heads), jnp.bfloat16),
            jax.ShapeDtypeStruct((ROPE, length), jnp.bfloat16),
            jax.ShapeDtypeStruct((1, heads), jnp.bfloat16),
        ),
        in_specs=[vmem] * 5,
        out_specs=(any_space, any_space, any_space, vmem),
        scratch_shapes=[dma((3,))],
        compiler_params=pltpu.CompilerParams(vmem_limit_bytes=24 * 1024 * 1024),
        name="attend",
    )(keys, values, rope, q_nope, q_rope)


def solution(mesh):
    n_sp, n_tp = mesh.shape["sp"], mesh.shape["tp"]

    def body(*args):
        keys, values, rope, read = local(n_sp, n_tp, *args)
        return keys[None], values[None], rope[None], read

    in_specs = (
        P(("grp", "tp"), "sp", None),
        P(("grp", "tp")),
        P(),
        P("sp", None),
        P(),
        P(),
        P(None, "tp"),
        P(None, "tp"),
        P(("grp", "sp"), "tp"),
        P(("grp", "sp"), "tp"),
    )
    out_specs = (
        P(("grp", "sp"), None, "tp"),
        P(("grp", "sp"), None, "tp"),
        P(("grp", "sp"), None, None),
        P(("grp", "sp"), "tp"),
    )
    return jax.shard_map(body, mesh=mesh, in_specs=in_specs, out_specs=out_specs, check_vma=False)
```

time: 517 us -> 268 us (0.52)
  waiting for transfers between devices: 392 us -> 0 us
  Pallas kernels: 0 us -> 259 us
  local copies, waits for them, and re-layouts: 41 us -> 7.72 us
  starting transfers between devices: 28.8 us -> 0 us
  matrix products: 23.8 us -> 0 us
  between operations: 14.2 us -> 0.68 us
  other arithmetic: 13.5 us -> 0 us
    pallas_call x0 -> x2, Pallas kernels: none -> 259 us  [the longest x1 256 us: local(): pl.pallas_call(functools.partial(exchange, n_sp, n_tp), out_shape=(jax.Sh...]
    all_to_all x4 -> x0, waiting for transfers between devices: 241 us -> none  [the longest x1 181 us: local(): lax.all_to_all(by_head[:, :, None], 'sp', split_axis=1, concat_axis=2, ti...]
    all_gather x2 -> x0, waiting for transfers between devices: 150 us -> none  [the longest x1 95.7 us: local(): lax.all_gather(w_latent, 'sp', axis=0, tiled=True)]
    all_to_all x4 -> x0, starting transfers between devices: 28.7 us -> none  [the longest x1 12 us: local(): lax.all_to_all(rope_every[None, :, None], 'sp', split_axis=1, concat_axis...]
    dot_general x6 -> x0, matrix products: 23.8 us -> none  [the longest x1 9.62 us: local(): jnp.einsum('tk,skc->stc', latent, lax.all_gather(paired, 'tp', axis=2, ti...]
    reshape x4 -> x0, local copies, waits for them, and re-layouts: 12 us -> none  [the longest x1 11.2 us: local(): both = both.reshape(2, prompts, rows, both.shape[2])]
    slice x3 -> x0, local copies, waits for them, and re-layouts: 7.6 us -> none  [the longest x2 5.1 us: local(): values = moved[1].reshape(length, head_cols)]
    another operation x2 -> x0, local copies, waits for them, and re-layouts: 6.67 us -> none  [the longest x1 4.33 us: local(): keys_split = keys.reshape(length, heads_here, HEAD)]
  transfers between devices with their start and end apart: 6 -> 0, of which waited for: 5 -> 0; matrix products, arithmetic and copies ran while one was open for 10% -> 0% of each run, Pallas kernels for 0% -> 0%
where the time goes in v1:
time: 268 us
  Pallas kernels  259 us (97%)
  local copies, waits for them, and re-layouts  7.72 us (3%)
    pallas_call x1, Pallas kernels, local(): pl.pallas_call(functools.partial(exchange, n_sp, n_tp), out_shape=(jax.Sh...  256 us
    unnamed x20, local copies, waits for them, and re-layouts  7.72 us

profile of v1, /device:TPU:163, one launch (start us, length us, event | category | flops | bytes accessed | tf_op | source)
XLA Modules:
  0.0 267.8 jit_solution(8055763426850085456)
XLA Ops:
  0.6 0.0 copy-start.1
  0.6 1.0 copy-done.1
  1.7 0.0 copy-start.2
  1.7 1.0 copy-done.2
  2.7 0.0 copy-start.3
  2.7 1.0 copy-done.3
  3.8 0.0 copy-start.4
  3.8 0.9 copy-done.4
  4.7 0.0 copy-start.5
  4.7 0.7 copy-done.5
  5.4 0.0 copy-start.6
  5.4 0.7 copy-done.6
  6.1 0.0 copy-start.8
  6.1 0.7 copy-done.8
  6.8 0.0 copy-start.7
  6.8 0.0 copy-start.9
  6.8 256.4 %exchange.1 = (bf16[4096,256]{1,0:T(8,128)(2,1)S(1)}, bf16[4096,256]{1,0:T(8,128)(2,1)}, bf16[32,4096]{1,0:T(8,128)(2,1)S(1)}) custom-call(bf16[512,4096]{1,0:T(8,128)(2,1)} %bitcast.10, s32[2]{0:T(128)S(1)} %copy-done.8, f32[1,4096]{1,0:T(1,128)S(1)} %bitcast.8, bf16[256,1024]{1,0:T(8,128)(2,1)S(1)} %copy-done.1, bf16[32,4096]{1,0:T(8,128)(2,1)S(1)} %bitcast.7, ...), custom_call_target="tpu_custom_call" | custom-call | tf_op jit(solution)/shard_map/exchange/pallas_call | solution.py:412
  263.2 0.0 copy-done.7
  263.2 0.0 copy-done.9
  263.3 0.0 copy-start
  263.3 1.6 copy-done
  264.8 2.9 %attend.1 = (bf16[4096,256]{1,0:T(8,128)(2,1)}, bf16[4096,256]{1,0:T(8,128)(2,1)}, bf16[32,4096]{1,0:T(8,128)(2,1)}, bf16[1,256]{1,0:T(2,128)(2,1)}) custom-call(bf16[4096,256]{1,0:T(8,128)(2,1)S(1)} %get-tuple-element.11.keys_ref, bf16[4096,256]{1,0:T(8,128)(2,1)S(1)} %copy-done, bf16[32,4096]{1,0:T(8,128)(2,1)S(1)} %get-tuple-element.13.rope_ref, ...), custom_call_target="tpu_custom_call" | custom-call | tf_op jit(solution)/shard_map/attend/pallas_call | solution.py:449
Async XLA Ops:
  0.6 1.0 copy-start.1
  1.7 1.0 copy-start.2
  2.7 1.0 copy-start.3
  3.8 0.9 copy-start.4
  4.7 0.7 copy-start.5
  5.4 0.7 copy-start.6
  6.1 0.7 copy-start.8
  6.8 256.5 %copy-start.7 = (bf16[1,256]{1,0:T(2,128)(2,1)S(1)}, bf16[1,256]{1,0:T(2,128)(2,1)}, u32[]{:S(2)}) copy-start(bf16[1,256]{1,0:T(2,128)(2,1)} %qn_ref.1) | copy-start | bytes 1540
  6.8 256.5 %copy-start.9 = (bf16[1,128]{1,0:T(2,128)(2,1)S(1)}, bf16[1,128]{1,0:T(2,128)(2,1)}, u32[]{:S(2)}) copy-start(bf16[1,128]{1,0:T(2,128)(2,1)} %qr_ref.1) | copy-start | bytes 772
  263.3 1.6 copy-start

commit v2 on v1

v2 whole, which is shorter than its diff:
```python
import functools

import jax
import jax.numpy as jnp
from jax import lax
from jax.experimental import pallas as pl
from jax.experimental.pallas import tpu as pltpu
from jax.sharding import PartitionSpec as P

HEAD = 64
ROPE = 32
EPS = 1e-06
MESH = pl.DeviceIdType.MESH
FULL = 48

HALVES = 2


def exchange(
    n_sp, n_tp, tok_hbm, off_ref, gain_hbm, wl_hbm, wrope_hbm, kvg_hbm, wk_hbm, wv_hbm,
    keys_ref, values_ref, rope_ref,
    norm, wfull, wup, lat, acc, latall, ropeown, stage, gain_ref, wrope_ref, kvg_ref,
    local_sem, wz_sem, wx_sem, wp_sem, wsend, a_sem, dir_sem, lx_sem, lp_sem, lsend, rsem, rsend,
):
    z = lax.axis_index("sp")
    t = lax.axis_index("tp")
    n_x = n_tp // 2
    x, c = t // 2, lax.rem(t, 2)
    rows = norm.shape[0] // 2
    width = norm.shape[1]
    rank = lat.shape[1]
    depth = width // n_sp
    half = depth // 2
    quarter = rank // n_x
    piece = rows // n_x
    heads = keys_ref.shape[1]

    def wrap(v, n):
        return lax.rem(v + 2 * n, n)

    def dev(xx, cc, zz):
        return {"sp": zz, "tp": 2 * xx + cc}

    z_next, z_prev = wrap(z + 1, n_sp), wrap(z - 1, n_sp)
    right = dev(wrap(x + 1, n_x), c, z)
    left = dev(wrap(x - 1, n_x), c, z)
    up = dev(x, c, z_next)
    down = dev(x, c, z_prev)
    partner = dev(x, 1 - c, z)
    home = lax.rem(z, 2)
    src_x, src_c = z // 4, lax.rem(z // 2, 2)
    has_self = jnp.logical_and(src_c == c, c == home)

    loads = [
        pltpu.make_async_copy(wl_hbm, wfull.at[pl.ds(z * depth, depth)], local_sem.at[0]),
        pltpu.make_async_copy(tok_hbm, norm, local_sem.at[1]),
        pltpu.make_async_copy(wk_hbm, wup.at[:, pl.ds(0, heads)], local_sem.at[2]),
        pltpu.make_async_copy(wv_hbm, wup.at[:, pl.ds(heads, heads)], local_sem.at[3]),
        pltpu.make_async_copy(gain_hbm, gain_ref, local_sem.at[4]),
        pltpu.make_async_copy(wrope_hbm, wrope_ref, local_sem.at[5]),
        pltpu.make_async_copy(kvg_hbm, kvg_ref, local_sem.at[6]),
    ]
    for load in loads:
        load.start()

    barrier = pltpu.get_barrier_semaphore()

    def greet(device):
        pl.semaphore_signal(barrier, inc=1, device_id=device, device_id_type=MESH)

    column = lax.rem(z // 2, n_x)
    rope_self = jnp.logical_and(jnp.logical_and(x == src_x, c == src_c), jnp.logical_and(x == column, c == home))
    around = (right, left, up, down, partner)
    for device in around:
        greet(device)
    pl.semaphore_wait(barrier, len(around))

    def send(src, dst, device, send_sem, recv_sem):
        pltpu.make_async_remote_copy(
            src_ref=src, dst_ref=dst, send_sem=send_sem, recv_sem=recv_sem,
            device_id=device, device_id_type=MESH,
        ).start()

    def arrived(dst, recv_sem):
        pltpu.make_async_copy(dst, dst, recv_sem).wait()

    def w_full(s):
        return wfull.at[pl.ds(s * depth + c * half, FULL)]

    def w_part(s, xx):
        return wfull.at[
            pl.ds(s * depth + c * half + FULL, half - FULL), pl.ds(pl.multiple_of(xx * quarter, quarter), quarter)
        ]

    def w_half(s, cc):
        return wfull.at[pl.ds(s * depth + cc * half, half)]

    steps = n_sp // 2
    limit = {("f", 1): steps, ("f", -1): steps - 1, ("q", 1): steps - 1, ("q", -1): steps}

    def z_send(kind, sign, k):
        s = wrap(z - sign * k, n_sp)
        ref = w_full(s) if kind == "f" else w_part(s, x)
        row = ("f", "q").index(kind) * 2 + (sign < 0)
        send(ref, ref, up if sign > 0 else down, wsend.at[row], wz_sem.at[row, k])

    def z_arrive(kind, sign, k):
        s = wrap(z - sign * k, n_sp)
        ref = w_full(s) if kind == "f" else w_part(s, x)
        row = ("f", "q").index(kind) * 2 + (sign < 0)
        arrived(ref, wz_sem.at[row, k - 1])
        if k < limit[kind, sign]:
            z_send(kind, sign, k)
        if kind == "q":
            col = k - 1 if sign > 0 else steps + k - 2
            send(ref, ref, right, wsend.at[4], wx_sem.at[0, col])
            send(ref, ref, left, wsend.at[5], wx_sem.at[1, col])

    def x_arrive(sign, k):
        s = wrap(z - sign * k, n_sp)
        col = k - 1 if sign > 0 else steps + k - 2
        from_left, from_right = w_part(s, wrap(x - 1, n_x)), w_part(s, wrap(x + 1, n_x))
        arrived(from_left, wx_sem.at[0, col])
        if sign > 0:
            send(from_left, from_left, right, wsend.at[6], wx_sem.at[2, col])
        arrived(from_right, wx_sem.at[1, col])
        if sign < 0:
            send(from_right, from_right, left, wsend.at[6], wx_sem.at[2, col])

    def far_arrive(sign, k):
        s = wrap(z - sign * k, n_sp)
        col = k - 1 if sign > 0 else steps + k - 2
        far = w_part(s, wrap(x + 2, n_x))
        arrived(far, wx_sem.at[2, col])
        ref = w_half(s, c)
        send(ref, ref, partner, wsend.at[7], wp_sem.at[col])

    loads[0].wait()
    if True:
        for kind in ("f", "q"):
            for sign in (1, -1):
                z_send(kind, sign, 0)

    loads[1].wait()
    loads[4].wait()
    loads[5].wait()
    loads[6].wait()

    def normalise(part, parts):
        @pl.loop(part * 2 * rows // 16 // parts, (part + 1) * 2 * rows // 16 // parts)
        def _(n):
            r = pl.ds(pl.multiple_of(n * 16, 16), 16)
            wide = norm[r, :].astype(jnp.float32)
            scale = lax.rsqrt(jnp.sum(wide * wide, axis=-1, keepdims=True) * (1.0 / width) + EPS)
            norm[r, :] = (wide * scale * gain_ref[...]).astype(jnp.bfloat16)

    def partial(s, first=False):
        @pl.loop(0, n_x)
        def _(n):
            cols = pl.ds(pl.multiple_of(n * quarter, quarter), quarter)
            term = jnp.dot(
                norm[:, pl.ds(pl.multiple_of(s * depth, depth), depth)],
                wfull[pl.ds(pl.multiple_of(s * depth, depth), depth), cols],
                preferred_element_type=jnp.float32,
            )
            acc[:, cols] = term if first else acc[:, cols] + term

    def finish(sign, k):
        s = wrap(z - sign * k, n_sp)
        col = k - 1 if sign > 0 else steps + k - 2
        arrived(w_half(s, 1 - c), wp_sem.at[col])
        partial(s)

    def rotary():
        raw = lax.dot_general(
            wrope_ref[...], norm[...], (((1,), (1,)), ((), ())), preferred_element_type=jnp.float32
        )
        index = lax.broadcasted_iota(jnp.int32, (ROPE // 2, rows), 0).astype(jnp.float32) * 2.0
        inverse = jnp.exp(index * (-jnp.log(jnp.float32(10000.0)) / ROPE))
        place = lax.broadcasted_iota(jnp.int32, (ROPE // 2, rows), 1)
        for j in range(2):
            angle = (off_ref[j] + z * rows + place).astype(jnp.float32) * inverse
            cosine, sine = jnp.cos(angle), jnp.sin(angle)
            first = raw[: ROPE // 2, j * rows:(j + 1) * rows]
            second = raw[ROPE // 2:, j * rows:(j + 1) * rows]
            ropeown[j] = jnp.concatenate(
                [first * cosine - second * sine, second * cosine + first * sine], axis=0
            ).astype(jnp.bfloat16)

    normalise(0, 4)
    if True:
        for k in range(1, steps + 1):
            for sign in (1, -1):
                for kind in ("q", "f"):
                    if k <= limit[kind, sign]:
                        z_arrive(kind, sign, k)
            if k < 4:
                normalise(k, 4)
            for sign in (1, -1):
                if 1 <= k - 1 <= limit["q", sign]:
                    x_arrive(sign, k - 1)
            for sign in (1, -1):
                if 1 <= k - 2 <= limit["q", sign]:
                    far_arrive(sign, k - 2)
            if k == 3:
                partial(z, True)
            if k == 4:
                rotary()
            for sign in (1, -1):
                if 1 <= k - 3:
                    finish(sign, k - 3)
        x_arrive(-1, steps)
        for sign in (1, -1):
            far_arrive(sign, steps - 1)
        for sign in (1, -1):
            finish(sign, steps - 2)
        far_arrive(-1, steps)
        for sign in (1, -1):
            finish(sign, steps - 1)
        finish(-1, steps)

    for j in range(2):
        own = jnp.logical_and(rope_self, 2 * t + j == z)
        dst = rope_ref.at[:, pl.ds(pl.multiple_of(z * rows, rows), rows)]

        @pl.when(own)
        def _():
            pltpu.make_async_copy(ropeown.at[j], dst, rsem.at[z]).start()

        @pl.when(jnp.logical_not(own))
        def _():
            send(ropeown.at[j], dst, dev(column, home, 2 * t + j), rsend.at[0, j], rsem.at[z])

    small = piece // HALVES

    def own_piece(j, q, h):
        return lat.at[pl.ds(pl.multiple_of(j * rows + q * piece + h * small, small), small)]

    def staged(xx, j, h):
        return stage.at[xx, j, pl.ds(h * small, small)]

    def place_of(s, q, h):
        return latall.at[pl.ds(pl.multiple_of(s * rows + q * piece + h * small, small), small)]

    for j in range(2):
        @pl.loop(j * rows // 16, (j + 1) * rows // 16)
        def _(n):
            r = pl.ds(pl.multiple_of(n * 16, 16), 16)
            wide = acc[r, :]
            scale = lax.rsqrt(jnp.sum(wide * wide, axis=-1, keepdims=True) * (1.0 / rank) + EPS)
            lat[r, :] = (wide * scale * kvg_ref[...]).astype(jnp.bfloat16)

        stage[x, j] = lat[pl.ds(pl.multiple_of(j * rows + x * piece, piece), piece), :]
        for h in range(HALVES):
            for d in (2, 1, -1):
                q = wrap(x + d, n_x)
                send(own_piece(j, q, h), staged(x, j, h), dev(q, c, z), lsend.at[0, j], a_sem.at[x, j, h])

    origin = lax.rem(z - 2 * c + n_sp, n_sp) // 4
    for d in (0, 1, -1, 2):
        xx = wrap(origin + d, n_x)
        for j in range(2):
            goal = 4 * xx + 2 * c + j
            own = jnp.logical_and(has_self, goal == z)
            for h in range(HALVES):
                @pl.when(xx != x)
                def _():
                    arrived(staged(xx, j, h), a_sem.at[xx, j, h])

                src, dst, sem = staged(xx, j, h), place_of(z, x, h), dir_sem.at[z // 2, h]

                @pl.when(own)
                def _():
                    pltpu.make_async_copy(src, dst, sem).start()

                @pl.when(jnp.logical_not(own))
                def _():
                    send(src, dst, dev(x, home, goal), lsend.at[3, 0], sem)

    near = [0] + [v for k in range(2, steps, 2) for v in (k, -k)] + [steps]
    odd = [v for k in range(1, steps, 2) for v in (k, -k)]
    same = home == c
    sources = [wrap(z + jnp.where(same, a, b), n_sp) for a, b in zip(near, odd)]
    other = [wrap(z + jnp.where(same, b, a), n_sp) for a, b in zip(near, odd)]
    n_src = len(sources)

    def direct(n, h):
        s = sources[n]
        ref = place_of(s, x, h)
        arrived(ref, dir_sem.at[s // 2, h])
        send(ref, ref, right, lsend.at[1, 0], lx_sem.at[0, n, h])
        send(ref, ref, left, lsend.at[1, 1], lx_sem.at[1, n, h])

    def beside(n, h):
        s = sources[n]
        from_left, from_right = place_of(s, wrap(x - 1, n_x), h), place_of(s, wrap(x + 1, n_x), h)
        arrived(from_left, lx_sem.at[0, n, h])
        if (n + h) % 2 == 0:
            send(from_left, from_left, right, lsend.at[2, 0], lx_sem.at[2, n, h])
        arrived(from_right, lx_sem.at[1, n, h])
        if (n + h) % 2 == 1:
            send(from_right, from_right, left, lsend.at[2, 0], lx_sem.at[2, n, h])

    def block(s):
        return latall.at[pl.ds(pl.multiple_of(s * rows, rows), rows)]

    def far(n, h):
        s = sources[n]
        arrived(place_of(s, wrap(x + 2, n_x), h), lx_sem.at[2, n, h])
        if h == HALVES - 1:
            send(block(s), block(s), partner, lsend.at[2, 1], lp_sem.at[s])

    def up_project(s):
        r = pl.ds(pl.multiple_of(s * rows, rows), rows)
        both = jnp.dot(latall[r, :], wup[...], preferred_element_type=jnp.float32).astype(jnp.bfloat16)
        keys_ref[r, :] = both[:, :heads]
        values_ref[r, :] = both[:, heads:]

    def rope_block(s):
        return rope_ref.at[:, pl.ds(pl.multiple_of(s * rows, rows), rows)]

    peers = [(dx, dc) for dx in range(n_x) for dc in range(2) if dx or dc]
    def rope_onward():
        for g in range(n_sp // 2 // n_x):
            s = 2 * (x + n_x * g) + c
            arrived(rope_block(s), rsem.at[s])
            for n, (dx, dc) in enumerate(peers):
                send(
                    rope_block(s), rope_block(s), dev(wrap(x + dx, n_x), lax.rem(c + dc, 2), z),
                    rsend.at[1 + g, n], rsem.at[s],
                )

    loads[2].wait()
    loads[3].wait()
    order = [(n, h) for n in range(n_src) for h in range(HALVES)]
    for i in range(len(order) + 2):
        if i < len(order):
            direct(*order[i])
        if 1 <= i <= len(order):
            beside(*order[i - 1])
        if i == 6:
            rope_onward()
        if 2 <= i:
            far(*order[i - 2])
            n, h = order[i - 2]
            if h == HALVES - 1:
                up_project(sources[n])
            elif n >= 1:
                arrived(block(other[n - 1]), lp_sem.at[other[n - 1]])
                up_project(other[n - 1])
    arrived(block(other[n_src - 1]), lp_sem.at[other[n_src - 1]])
    up_project(other[n_src - 1])

    for s in range(n_sp):
        mine = jnp.logical_and(lax.rem(s // 2, n_x) == x, s % 2 == c)

        @pl.when(jnp.logical_not(mine))
        def _():
            arrived(rope_block(s), rsem.at[s])

    for j in range(2):
        own = jnp.logical_and(rope_self, 2 * t + j == z)

        @pl.when(jnp.logical_not(own))
        def _():
            arrived(ropeown.at[j], rsend.at[0, j])

    for g in range(n_sp // 2 // n_x):
        for n in range(len(peers)):
            arrived(ropeown.at[0], rsend.at[1 + g, n])
    if True:
        for sign in (1, -1):
            for _ in range(1):
                f_rows, q_rows = limit["f", sign] * FULL, limit["q", sign] * (half - FULL)
                arrived(wfull.at[pl.ds(0, f_rows)], wsend.at[int(sign < 0)])
                arrived(wfull.at[pl.ds(0, q_rows), pl.ds(0, quarter)], wsend.at[2 + int(sign < 0)])
        q_rows = (2 * steps - 1) * (half - FULL)
        for row in (4, 5, 6):
            arrived(wfull.at[pl.ds(0, q_rows), pl.ds(0, quarter)], wsend.at[row])
        arrived(wfull.at[pl.ds(0, (2 * steps - 1) * half)], wsend.at[7])
    if True:
        for j in range(2):
            arrived(lat.at[pl.ds(0, rows - piece)], lsend.at[0, j])
        pl.when(has_self)(lambda: arrived(lat.at[pl.ds(0, 2 * rows - piece)], lsend.at[3, 0]))
        pl.when(jnp.logical_not(has_self))(lambda: arrived(lat, lsend.at[3, 0]))
        for a, b in ((1, 0), (1, 1), (2, 0)):
            arrived(latall.at[pl.ds(0, n_src * piece)], lsend.at[a, b])
        arrived(latall.at[pl.ds(0, n_src * rows)], lsend.at[2, 1])


def in_hbm(value):
    return pltpu.with_memory_space_constraint(value, pltpu.HBM)


def attend(
    keys_ref, values_ref, rope_ref, qn_ref, qr_ref, keys_out, values_out, rope_out, read_ref, sem
):
    outs = [
        pltpu.make_async_copy(keys_ref, keys_out, sem.at[0]),
        pltpu.make_async_copy(values_ref, values_out, sem.at[1]),
        pltpu.make_async_copy(rope_ref, rope_out, sem.at[2]),
    ]
    for out in outs:
        out.start()
    heads = keys_ref.shape[1] // HEAD
    rot = qr_ref.shape[1] // heads
    pad = 8

    def by_head(ref, size):
        wide = jnp.broadcast_to(ref[...].astype(jnp.float32), (pad, ref.shape[1]))
        row = lax.broadcasted_iota(jnp.int32, wide.shape, 0)
        col = lax.broadcasted_iota(jnp.int32, wide.shape, 1)
        return jnp.where(col // size == row, wide, 0.0)

    nope = by_head(qn_ref, HEAD).astype(jnp.bfloat16)
    scores = lax.dot_general(
        nope, keys_ref[...], (((1,), (1,)), ((), ())), preferred_element_type=jnp.float32
    )
    spread = by_head(qr_ref, rot)
    rotary = spread[:, :rot]
    for h in range(1, heads):
        rotary = rotary + spread[:, h * rot:(h + 1) * rot]
    scores = scores + jnp.dot(
        rotary.astype(jnp.bfloat16), rope_ref[...], preferred_element_type=jnp.float32
    )
    scores = scores / jnp.sqrt(jnp.float32(HEAD + ROPE))
    expo = jnp.exp(scores - jnp.max(scores, axis=-1, keepdims=True))
    weights = (expo / jnp.sum(expo, axis=-1, keepdims=True)).astype(jnp.bfloat16)
    read = jnp.dot(weights, values_ref[...], preferred_element_type=jnp.float32)
    row = lax.broadcasted_iota(jnp.int32, read.shape, 0)
    col = lax.broadcasted_iota(jnp.int32, read.shape, 1)
    read_ref[...] = jnp.sum(
        jnp.where(col // HEAD == row, read, 0.0), axis=0, keepdims=True
    ).astype(jnp.bfloat16)
    for out in outs:
        out.wait()


def local(
    n_sp, n_tp,
    tokens, offsets, in_gain, w_latent, w_rope_key, kv_gain, w_up_key, w_up_value, q_nope, q_rope
):
    prompts, rows, width = tokens.shape
    depth, rank = w_latent.shape
    heads = w_up_key.shape[1]
    length = n_sp * rows
    steps = n_sp // 2
    any_space = pl.BlockSpec(memory_space=pl.ANY)
    hbm = pl.BlockSpec(memory_space=pltpu.HBM)
    vmem = pl.BlockSpec(memory_space=pltpu.VMEM)
    smem = pl.BlockSpec(memory_space=pltpu.SMEM)
    dma = pltpu.SemaphoreType.DMA
    keys, values, rope = pl.pallas_call(
        functools.partial(exchange, n_sp, n_tp),
        out_shape=(
            jax.ShapeDtypeStruct((length, heads), jnp.bfloat16),
            jax.ShapeDtypeStruct((length, heads), jnp.bfloat16),
            jax.ShapeDtypeStruct((ROPE, length), jnp.bfloat16),
        ),
        in_specs=[hbm, smem, hbm, hbm, hbm, hbm, hbm, hbm],
        out_specs=(vmem, vmem, vmem),
        scratch_shapes=[
            pltpu.VMEM((prompts * rows, width), jnp.bfloat16),
            pltpu.VMEM((width, rank), jnp.bfloat16),
            pltpu.VMEM((rank, 2 * heads), jnp.bfloat16),
            pltpu.VMEM((prompts * rows, rank), jnp.bfloat16),
            pltpu.VMEM((prompts * rows, rank), jnp.float32),
            pltpu.VMEM((length, rank), jnp.bfloat16),
            pltpu.VMEM((prompts, ROPE, rows), jnp.bfloat16),
            pltpu.VMEM((n_tp // 2, prompts, rows * 2 // n_tp, rank), jnp.bfloat16),
            pltpu.VMEM((1, width), jnp.float32),
            pltpu.VMEM((ROPE, width), jnp.bfloat16),
            pltpu.VMEM((1, rank), jnp.float32),
            dma((7,)),
            dma((4, steps)),
            dma((3, 2 * steps - 1)),
            dma((2 * steps - 1,)),
            dma((8,)),
            dma((n_tp // 2, prompts, HALVES)),
            dma((steps, HALVES)),
            dma((3, steps, HALVES)),
            dma((n_sp,)),
            dma((4, 2)),
            dma((n_sp,)),
            dma((1 + n_sp // n_tp, n_tp - 1)),
        ],
        compiler_params=pltpu.CompilerParams(
            collective_id=0, has_side_effects=True, vmem_limit_bytes=40 * 1024 * 1024
        ),
        name="exchange",
    )(
        *map(
            in_hbm,
            (tokens.reshape(prompts * rows, width),),
        ),
        offsets,
        *map(
            in_hbm,
            (
                in_gain.reshape(1, width), w_latent, w_rope_key.T, kv_gain.reshape(1, rank),
                w_up_key, w_up_value,
            ),
        ),
    )
    return pl.pallas_call(
        attend,
        out_shape=(
            jax.ShapeDtypeStruct((length, heads), jnp.bfloat16),
            jax.ShapeDtypeStruct((length, heads), jnp.bfloat16),
            jax.ShapeDtypeStruct((ROPE, length), jnp.bfloat16),
            jax.ShapeDtypeStruct((1, heads), jnp.bfloat16),
        ),
        in_specs=[vmem] * 5,
        out_specs=(any_space, any_space, any_space, vmem),
        scratch_shapes=[dma((3,))],
        compiler_params=pltpu.CompilerParams(vmem_limit_bytes=24 * 1024 * 1024),
        name="attend",
    )(keys, values, rope, q_nope, q_rope)


def solution(mesh):
    n_sp, n_tp = mesh.shape["sp"], mesh.shape["tp"]

    def body(*args):
        keys, values, rope, read = local(n_sp, n_tp, *args)
        return keys[None], values[None], rope[None], read

    in_specs = (
        P(("grp", "tp"), "sp", None),
        P(("grp", "tp")),
        P(),
        P("sp", None),
        P(),
        P(),
        P(None, "tp"),
        P(None, "tp"),
        P(("grp", "sp"), "tp"),
        P(("grp", "sp"), "tp"),
    )
    out_specs = (
        P(("grp", "sp"), None, "tp"),
        P(("grp", "sp"), None, "tp"),
        P(("grp", "sp"), None, None),
        P(("grp", "sp"), "tp"),
    )
    return jax.shard_map(body, mesh=mesh, in_specs=in_specs, out_specs=out_specs, check_vma=False)
```

time: 268 us -> 171 us (0.64); the launches traced: 268 us -> 168 us
  Pallas kernels: 259 us -> 166 us
  local copies, waits for them, and re-layouts: 7.72 us -> 0.66 us
    pallas_call x1, Pallas kernels: 256 us -> 163 us  [local(): pl.pallas_call(functools.partial(exchange, n_sp, n_tp), out_shape=(jax.Sh...]
    unnamed x20 -> x6, local copies, waits for them, and re-layouts: 7.72 us -> 0.66 us
where the time goes in v2:
time: 171 us; the launch traced here: 168 us
  Pallas kernels  166 us (97%)
    pallas_call x1, Pallas kernels, local(): pl.pallas_call(functools.partial(exchange, n_sp, n_tp), out_shape=(jax.Sh...  163 us

profile of v2, /device:TPU:163, one launch (start us, length us, event | category | flops | bytes accessed | tf_op | source)
XLA Modules:
  0.0 167.9 jit_solution(11924258758311835954)
XLA Ops:
  0.6 0.0 copy-start.1
  0.6 0.6 copy-done.1
  1.3 0.0 copy-start
  1.3 0.0 copy-start.2
  1.3 163.5 %exchange.1 = (bf16[4096,256]{1,0:T(8,128)(2,1)S(1)}, bf16[4096,256]{1,0:T(8,128)(2,1)S(1)}, bf16[32,4096]{1,0:T(8,128)(2,1)S(1)}) custom-call(bf16[512,4096]{1,0:T(8,128)(2,1)} %bitcast.7, s32[2]{0:T(128)S(1)} %copy-done.1, f32[1,4096]{1,0:T(1,128)} %bitcast.9, bf16[256,1024]{1,0:T(8,128)(2,1)} %wl_hbm.1, bf16[32,4096]{1,0:T(8,128)(2,1)} %bitcast.8, ...), custom_call_target="tpu_custom_call" | custom-call | tf_op jit(solution)/shard_map/exchange/pallas_call | solution.py:453
  164.8 0.0 copy-done
  164.8 0.0 copy-done.2
  164.8 2.9 %attend.1 = (bf16[4096,256]{1,0:T(8,128)(2,1)}, bf16[4096,256]{1,0:T(8,128)(2,1)}, bf16[32,4096]{1,0:T(8,128)(2,1)}, bf16[1,256]{1,0:T(2,128)(2,1)}) custom-call(bf16[4096,256]{1,0:T(8,128)(2,1)S(1)} %get-tuple-element.11.keys_ref, bf16[4096,256]{1,0:T(8,128)(2,1)S(1)} %get-tuple-element.12.values_ref, bf16[32,4096]{1,0:T(8,128)(2,1)S(1)} %get-tuple-element.13.rope_ref, ...), custom_call_target="tpu_custom_call" | custom-call | tf_op jit(solution)/shard_map/attend/pallas_call | solution.py:505
Async XLA Ops:
  0.6 0.7 copy-start.1
  1.3 163.5 %copy-start = (bf16[1,256]{1,0:T(2,128)(2,1)S(1)}, bf16[1,256]{1,0:T(2,128)(2,1)}, u32[]{:S(2)}) copy-start(bf16[1,256]{1,0:T(2,128)(2,1)} %qn_ref.1) | copy-start | bytes 1540
  1.3 163.5 %copy-start.2 = (bf16[1,128]{1,0:T(2,128)(2,1)S(1)}, bf16[1,128]{1,0:T(2,128)(2,1)}, u32[]{:S(2)}) copy-start(bf16[1,128]{1,0:T(2,128)(2,1)} %qr_ref.1) | copy-start | bytes 772
